TPU v7x, 32 devices: a whole 2x2x4 slice. The times are simulated.
32 devices in a mesh: sp: 16 (over z, y, x), tp: 2 (over core).
Axes of the slice: x: 2, y: 2, z: 4, core: 2. Of those that a mesh axis runs over, the one named last changes fastest.
Arguments:
- queries: bfloat16 [2048, 1024], P('sp', 'tp'), may hold values from -5 to 5
- keys: bfloat16 [2048, 1024], P('sp', 'tp'), may hold values from -5 to 5
- values: bfloat16 [2048, 1024], P('sp', 'tp'), may hold values from -5 to 5
- in_gate: float32 [8, 2048], P('tp', 'sp'), may hold values from -7 to 213
- forget_gate: float32 [8, 2048], P('tp', 'sp'), may hold values from 0 to 17
- stream: bfloat16 [2048, 2048], P('sp', 'tp'), may hold values from -24 to 24
- head_gain: float32 [1024], replicated, may hold values from 0.1 to 1.9
- out_weight: bfloat16 [1024, 2048], P(None, 'tp'), may hold values from -0.1875 to 0.1875
- norm_gain: float32 [2048], replicated, may hold values from 0.1 to 1.9
- gate_weight: bfloat16 [2048, 5632], P('sp', 'tp'), may hold values from -0.125 to 0.125
- up_weight: bfloat16 [2048, 5632], P('sp', 'tp'), may hold values from -0.125 to 0.125
- down_weight: bfloat16 [2048, 5632], P('sp', 'tp'), may hold values from -0.15625 to 0.15625
Outputs:
- layer_out: float32 [2048, 2048], P('sp', 'tp')
All inputs are finite; a program needn't handle non-finite values.
Results may differ from a plain program's by a relative error of at most 0.004.
Values may be sent and summed in bfloat16 or wider, within the bound.
A program may use at most 128 MiB of HBM per device.

v0:
```python
import jax
import jax.numpy as jnp
from jax import lax
from jax.sharding import PartitionSpec as P

D = 2048
HEAD_DIM = 128
BLOCK = 128


norm_eps = 1e-06
far_below = -1e30


def entering_2(array, axis, combine, identity):
    devices, here = (lax.axis_size(axis), lax.axis_index(axis))
    everything = jax.tree.map(lambda part: lax.all_gather(part, axis), array)
    start = jax.tree.map(
        lambda part, zero: jnp.broadcast_to(jnp.asarray(zero, part.dtype), part.shape),
        array,
        identity,
    )

    def step(k, before):
        reached = k < here
        new = combine(before, jax.tree.map(lambda part: part[k], everything))
        return jax.tree.map(lambda a, b: jnp.where(reached, a, b), new, before)

    return lax.fori_loop(0, devices, step, start)


def merge_states(earlier, later):
    memory_early, top_early, fall_early = earlier
    memory_late, top_late, fall_late = later
    new_top = jnp.maximum(fall_late + top_early, top_late)
    keep_early = jnp.exp(fall_late + top_early - new_top)
    keep_late = jnp.exp(top_late - new_top)
    memory = keep_early[..., None, None] * memory_early + keep_late[..., None, None] * memory_late
    return (memory, new_top, fall_early + fall_late)


def memory_cell(queries, keys, values, in_gate, forget_gate, own_gain):
    tokens = queries.shape[0]
    local_heads = in_gate.shape[0]
    blocks = tokens // BLOCK
    key_scale = HEAD_DIM ** (-0.5)
    query_blocks = queries.reshape(blocks, BLOCK, local_heads, HEAD_DIM)
    key_blocks = keys.reshape(blocks, BLOCK, local_heads, HEAD_DIM)
    value_blocks = values.reshape(blocks, BLOCK, local_heads, HEAD_DIM)
    gate_blocks = in_gate.reshape(local_heads, blocks, BLOCK)
    cumulative = jnp.cumsum(
        jax.nn.log_sigmoid(forget_gate).reshape(local_heads, blocks, BLOCK), axis=-1
    )
    block_fall = cumulative[..., -1]
    log_weight = block_fall[..., None] - cumulative + gate_blocks
    block_top = jnp.max(log_weight, axis=-1)
    key_weight = jnp.exp(log_weight - block_top[..., None]) * key_scale
    weighted = (jnp.transpose(key_weight, (1, 2, 0))[..., None] * key_blocks).astype(jnp.bfloat16)
    block_memory = jnp.einsum(
        "nshd,nshe->nhde", weighted, value_blocks, preferred_element_type=jnp.float32
    )
    neutral = (
        jnp.zeros((local_heads, HEAD_DIM, HEAD_DIM), jnp.float32),
        jnp.full((local_heads,), far_below, jnp.float32),
        jnp.zeros((local_heads,), jnp.float32),
    )

    def advance(running, summary):
        return (merge_states(running, summary), running)

    device_total, before_block = lax.scan(
        advance, neutral, (block_memory, block_top.T, block_fall.T)
    )
    incoming = entering_2(device_total, "sp", merge_states, neutral)
    start_state = (
        jnp.zeros((local_heads, HEAD_DIM, HEAD_DIM), jnp.float32),
        jnp.zeros((local_heads,), jnp.float32),
        jnp.zeros((local_heads,), jnp.float32),
    )
    entering = merge_states(start_state, incoming)
    memory_in, top_in, fall_in = merge_states(
        jax.tree.map(lambda member: member[None], entering), before_block
    )
    causal = lax.broadcasted_iota(jnp.int32, (BLOCK, BLOCK), 0) >= lax.broadcasted_iota(
        jnp.int32, (BLOCK, BLOCK), 1
    )
    spread = cumulative[..., :, None] - cumulative[..., None, :] + gate_blocks[..., None, :]
    spread = jnp.where(causal, spread, -jnp.inf)
    carried = cumulative + top_in.T[..., None]
    row_top = jnp.maximum(carried, jnp.max(spread, axis=-1))
    decay_weight = jnp.exp(spread - row_top[..., None])
    scores = jnp.einsum(
        "nthd,nshd->hnts", query_blocks, key_blocks, preferred_element_type=jnp.float32
    )
    weights = (scores * key_scale * decay_weight).astype(jnp.bfloat16)
    inner_part = jnp.einsum(
        "hnts,nshe->nthe", weights, value_blocks, preferred_element_type=jnp.float32
    )
    outer_part = jnp.einsum(
        "nthd,nhde->nthe",
        query_blocks.astype(jnp.float32),
        memory_in,
        precision=lax.Precision.HIGHEST,
    )
    readout = (
        jnp.transpose(jnp.exp(carried - row_top), (1, 2, 0))[..., None] * outer_part + inner_part
    )
    row_scale = lax.rsqrt(jnp.mean(readout * readout, axis=-1, keepdims=True) + norm_eps)
    head_scale = own_gain.reshape(local_heads, HEAD_DIM)
    normed_heads = (readout * row_scale * head_scale).astype(jnp.bfloat16)
    return normed_heads.reshape(tokens, local_heads * HEAD_DIM)


def local(
    queries,
    keys,
    values,
    in_gate,
    forget_gate,
    stream,
    head_gain,
    out_weight,
    norm_gain,
    gate_weight,
    up_weight,
    down_weight,
):
    column_index = lax.axis_index("tp")
    local_width = queries.shape[1]
    own_gain = lax.dynamic_slice_in_dim(head_gain, column_index * local_width, local_width)
    heads_out = memory_cell(queries, keys, values, in_gate, forget_gate, own_gain)
    columns = out_weight.shape[1]
    projected = jnp.dot(
        lax.all_gather(heads_out, "tp", axis=1, tiled=True),
        out_weight,
        preferred_element_type=jnp.float32,
    )
    mixed_stream = stream.astype(jnp.float32) + projected
    squares = lax.psum(jnp.sum(mixed_stream * mixed_stream, axis=1), "tp")
    factor = lax.rsqrt(squares / D + norm_eps)
    own_norm = lax.dynamic_slice_in_dim(norm_gain, column_index * columns, columns)
    own_normed = (mixed_stream * factor[:, None] * own_norm).astype(jnp.bfloat16)
    normed = lax.all_gather(own_normed, "tp", axis=1, tiled=True)
    gate_acts = jnp.dot(
        normed,
        lax.all_gather(gate_weight, "sp", axis=0, tiled=True),
        preferred_element_type=jnp.float32,
    )
    up_acts = jnp.dot(
        normed,
        lax.all_gather(up_weight, "sp", axis=0, tiled=True),
        preferred_element_type=jnp.float32,
    )
    hidden = (jax.nn.silu(gate_acts) * up_acts).astype(jnp.bfloat16)
    channel_terms = jnp.einsum(
        "df,tf->dt",
        lax.all_gather(down_weight, "sp", axis=0, tiled=True),
        hidden,
        preferred_element_type=jnp.float32,
    )
    channel = lax.psum_scatter(
        channel_terms.astype(jnp.bfloat16), "tp", scatter_dimension=0, tiled=True
    ).astype(jnp.float32)
    return mixed_stream + 0.5 * channel.T


def solution(mesh):
    return jax.shard_map(
        local,
        mesh=mesh,
        in_specs=(
            P("sp", "tp"),
            P("sp", "tp"),
            P("sp", "tp"),
            P("tp", "sp"),
            P("tp", "sp"),
            P("sp", "tp"),
            P(),
            P(None, "tp"),
            P(),
            P("sp", "tp"),
            P("sp", "tp"),
            P("sp", "tp"),
        ),
        out_specs=P("sp", "tp"),
        check_vma=False,
    )
```

profile of v0, /device:TPU:0, one launch (start us, length us, event | category | flops | bytes accessed | tf_op | source)
XLA Modules:
  0.0 548.2 jit_solution(9330180456237955510)
XLA Ops:
  6.5 0.0 all-gather.14.cloned.1.call-start
  6.6 0.8 fusion.42
  7.4 1.2 reduce_window_sum.13
  8.6 0.2 slice_reduce_fusion
  8.8 0.9 fusion.48
  9.7 0.8 multiply_bitcast_fusion
  10.4 0.1 copy.47
  10.5 0.2 multiply_reduce_fusion.2
  10.7 1.0 copy.59
  11.8 1.0 copy.60
  12.8 0.9 fusion.8
  13.7 0.0 all-gather.14.cloned.1.call-update
  13.7 0.0 all-gather.8.cloned.1.call-start
  13.8 0.7 all-gather.8.cloned.1.call-update
  14.5 0.0 all-gather.10.cloned.1.call-start
  14.5 0.7 all-gather.10.cloned.1.call-update
  15.2 0.0 all-gather.12.cloned.1.call-start
  15.3 0.5 all-gather.12.cloned.1.call-update
  15.8 0.0 reduce-scatter.2.cloned.1.call-start
  15.9 0.7 dynamic-slice.1
  17.3 0.2 dynamic-update-slice
  17.5 44.2 %all-reduce = f32[64]{0:T(128)S(1)} all-reduce(f32[64]{0:T(128)S(1)} %dynamic-update-slice), channel_id=2, replica_groups=mesh['sp'=16,'tp'=2] {'sp'}, use_global_device_ids=true, to_apply=%add | all-reduce | flops 64 | bytes 512
  61.7 0.1 reshape.230
  61.8 36.1 %all-gather.2 = f32[16,1,4]{2,1,0:T(1,128)S(1)} all-gather(f32[1,1,4]{2,1,0:T(1,128)S(1)} %fusion.44), channel_id=1, replica_groups=mesh['sp'=16,'tp'=2] {'sp'}, dimensions={0}, use_global_device_ids=true | all-gather | bytes 272 | tf_op jit(solution)/shard_map/all_gather | solution.py:17
  98.0 0.1 dynamic-slice_bitcast_fusion
  98.1 0.2 select_reduce_fusion
  98.3 0.0 all-gather.14.cloned.1.call-done
  98.3 0.0 copy-start.2
  98.3 18.3 %while.5 = (s32[]{:T(128)}, f32[4,128,128]{2,1,0:T(8,128)S(1)}, f32[4]{0:T(128)S(1)}, f32[4]{0:T(128)S(1)}, s32[]{:T(128)}, /*index=5*/f32[16,4]{1,0:T(8,128)S(1...) while((s32[]{:T(128)}, f32[4,128,128]{2,1,0:T(8,128)S(1)}, ...), condition=%wide.region_3.4_spmd.clone, body=%wide.region_2.3_spmd.clone.sunk | while | flops 327724 | bytes 786775 | solution.py:29
  98.4 1.1 fusion.65
  99.5 1.1 fusion.65
  100.7 1.1 fusion.65
  101.9 1.1 fusion.65
  103.0 1.1 fusion.65
  104.2 1.1 fusion.65
  105.3 1.1 fusion.65
  106.5 1.1 fusion.65
  107.6 1.1 fusion.65
  108.7 1.1 fusion.65
  109.9 1.1 fusion.65
  111.0 1.1 fusion.65
  112.2 1.1 fusion.65
  113.3 1.1 fusion.65
  114.5 1.1 fusion.65
  115.6 1.1 fusion.65
  116.7 0.1 add_maximum_fusion
  116.8 0.4 convolution_bitcast_fusion.1
  117.2 0.1 fusion.41
  117.2 0.5 multiply_reduce_fusion.1
  117.7 0.0 dynamic-slice-start
  117.8 0.1 multiply_convert_fusion.1
  117.9 2.0 all_gather.30
  119.9 0.5 multiply_reduce_fusion
  120.5 2.5 psum.7
  122.9 0.1 multiply_convert_fusion
  123.1 2.2 all_gather.31
  125.2 110.0 %all-gather.8.cloned.1.call-done = bf16[2048,2816]{1,0:T(8,128)(2,1)} async-done(((bf16[128,2816]{1,0:T(8,128)(2,1)}), bf16[2048,2816]{1,0:T(8,128)(2,1)}) %all-gather.8.cloned.1.call-update) | async-done | bytes 11534352 | tf_op jit(solution)/shard_map/all_gather | solution.py:146
  235.3 7.0 %fusion.51 = f32[128,2816]{1,0:T(8,128)} fusion(bf16[128,2048]{1,0:T(8,128)(2,1)S(1)} %all_gather.31, bf16[2048,2816]{1,0:T(8,128)(2,1)} %all-gather.8.cloned.1.call-done), kind=kOutput, calls=%fused_computation.91 | convolution fusion | flops 1476395008 | bytes 13500416 | tf_op jit(solution)/shard_map/dot_general | solution.py:144
  242.3 135.3 %all-gather.10.cloned.1.call-done = bf16[2048,2816]{1,0:T(8,128)(2,1)} async-done(((bf16[128,2816]{1,0:T(8,128)(2,1)}), bf16[2048,2816]{1,0:T(8,128)(2,1)}) %all-gather.10.cloned.1.call-update) | async-done | bytes 11534352 | tf_op jit(solution)/shard_map/all_gather | solution.py:151
  377.7 142.2 %all-gather.12.cloned.1.call-done = bf16[2048,2816]{1,0:T(8,128)(2,1)} async-done(((bf16[128,2816]{1,0:T(8,128)(2,1)}), bf16[2048,2816]{1,0:T(8,128)(2,1)}) %all-gather.12.cloned.1.call-update) | async-done | bytes 11534352 | tf_op jit(solution)/shard_map/all_gather | solution.py:157
  519.9 13.6 %fusion.6 = bf16[2048,128]{0,1:T(8,128)(2,1)} fusion(bf16[2048,2816]{1,0:T(8,128)(2,1)} %all-gather.12.cloned.1.call-done, bf16[128,2048]{1,0:T(8,128)(2,1)S(1)} %all_gather.31, bf16[2048,2816]{1,0:T(8,128)(2,1)} %all-gather.10.cloned.1.call-done, f32[128,2816]{1,0:T(8,128)} %fusion.51), kind=kOutput, calls=%fused_computation.17 | convolution fusion | flops 2955214848 | bytes 25559040 | tf_op jit(solution)/shard_map/df,tf->dt/dot_general | solution.py:155
  533.5 0.0 reduce-scatter.2.cloned.1.call-update
  533.6 6.3 %reduce-scatter.2.cloned.1.call-done = bf16[1024,128]{0,1:T(8,128)(2,1)} async-done(((bf16[2048,128]{0,1:T(8,128)(2,1)}), bf16[1024,128]{0,1:T(8,128)(2,1)}) %reduce-scatter.2.cloned.1.call-update) | async-done | bytes 262160 | tf_op jit(solution)/shard_map/reduce_scatter | solution.py:161
  539.8 1.8 bitcast_add_fusion
  (53 shorter events, 0.7 us)
Async XLA Ops:
  6.5 113.4 %copy-start = (bf16[1024,1024]{1,0:T(8,128)(2,1)S(1)}, bf16[1024,1024]{1,0:T(8,128)(2,1)}, u32[]{:S(2)}) copy-start(bf16[1024,1024]{1,0:T(8,128)(2,1)} %param.21) | copy-start | bytes 6291460
  6.5 9.4 %copy-start.5 = (u32[32]{0:T(128)S(1)}, u32[32]{0:T(128)}, u32[]{:S(2)}) copy-start(u32[32]{0:T(128)} %constant.87) | copy-start | bytes 388
  6.5 91.5 %copy-start.3 = (f32[4,128]{1,0:T(4,128)S(1)}, f32[4,128]{1,0:T(4,128)}, u32[]{:S(2)}) copy-start(f32[4,128]{1,0:T(4,128)} %param.17) | copy-start | bytes 6148
  6.5 91.4 %copy-start.4 = (f32[1024]{0:T(1024)S(1)}, f32[1024]{0:T(1024)}, u32[]{:S(2)}) copy-start(f32[1024]{0:T(1024)} %param.20) | copy-start | bytes 12292
  6.5 91.8 %all-gather.14.cloned.1.call-start = ((), (), s32[]{:S(2)}) async-start(), calls=%async_computation.5 | async-start | bytes 4456448 | tf_op jit(solution)/shard_map/all_gather | solution.py:17
  13.7 221.5 %all-gather.8.cloned.1.call-start = ((), (), s32[]{:S(2)}) async-start(), calls=%async_computation.1 | async-start | bytes 12255232 | tf_op jit(solution)/shard_map/all_gather | solution.py:146
  14.5 363.2 %all-gather.10.cloned.1.call-start = ((), (), s32[]{:S(2)}) async-start(), calls=%async_computation.2 | async-start | bytes 12255232 | tf_op jit(solution)/shard_map/all_gather | solution.py:151
  15.2 504.7 %all-gather.12.cloned.1.call-start = ((), (), s32[]{:S(2)}) async-start(), calls=%async_computation.3 | async-start | bytes 12255232 | tf_op jit(solution)/shard_map/all_gather | solution.py:157
  15.8 524.0 %reduce-scatter.2.cloned.1.call-start = ((), (), s32[]{:S(2)}) async-start(), calls=%async_computation.4 | async-start | bytes 786432 | tf_op jit(solution)/shard_map/reduce_scatter | solution.py:161
  98.3 18.5 %copy-start.2 = (bf16[128,512]{1,0:T(8,128)(2,1)S(1)}, bf16[128,512]{1,0:T(8,128)(2,1)}, u32[]{:S(2)}) copy-start(bf16[128,512]{1,0:T(8,128)(2,1)} %param.14) | copy-start | bytes 393220
  116.7 3.2 copy-start.1
  117.7 5.2 dynamic-slice-start
Sparse Core Ops, SparseCore 0:
  13.9 78.4 all-gather.13
  95.2 140.0 all-gather.7
  238.0 139.5 all-gather.9
  380.3 139.5 all-gather.11
  533.7 6.0 reduce-scatter.1
where the time goes:
time: 549 us; the launch traced here: 548 us
  waiting for transfers between devices  396 us (72%)
  blocking collectives  87 us (16%)
  other arithmetic  24.1 us (4%)
  matrix products  23 us (4%)
  between operations  14 us (3%)
    all_gather x1, waiting for transfers between devices, local(): lax.all_gather(down_weight, 'sp', axis=0, tiled=True)  142 us
    all_gather x1, waiting for transfers between devices, local(): lax.all_gather(up_weight, 'sp', axis=0, tiled=True)  135 us
    all_gather x1, waiting for transfers between devices, local(): lax.all_gather(gate_weight, 'sp', axis=0, tiled=True)  110 us
    unnamed x1, blocking collectives  44.2 us
    all_gather x1, blocking collectives, entering_2(): everything = jax.tree.map(lambda part: lax.all_gather(part, axis), array)  36.1 us
    select_n x32, other arithmetic, step(): return jax.tree.map(lambda a, b: jnp.where(reached, a, b), new, before)  17.5 us
    dot_general x1, matrix products, local(): jnp.einsum('df,tf->dt', lax.all_gather(down_weight, 'sp', axis=0, tiled=T...  13.6 us
  transfers between devices with their start and end apart: 5, of which 4 were waited for; matrix products, arithmetic and copies ran while one was open for 5% of the time, Pallas kernels for 0%

commit v1 on v0

--- a/solution.py
+++ b/solution.py
@@ -12,21 +12,31 @@
 far_below = -1e30
 
 
-def entering_2(array, axis, combine, identity):
-    devices, here = (lax.axis_size(axis), lax.axis_index(axis))
-    everything = jax.tree.map(lambda part: lax.all_gather(part, axis), array)
-    start = jax.tree.map(
-        lambda part, zero: jnp.broadcast_to(jnp.asarray(zero, part.dtype), part.shape),
-        array,
-        identity,
-    )
-
-    def step(k, before):
-        reached = k < here
-        new = combine(before, jax.tree.map(lambda part: part[k], everything))
-        return jax.tree.map(lambda a, b: jnp.where(reached, a, b), new, before)
-
-    return lax.fori_loop(0, devices, step, start)
+def entering_state(total):
+    memory, top, fall = total
+    devices, here = (lax.axis_size("sp"), lax.axis_index("sp"))
+    heads, rows, columns = memory.shape
+    own_tops = jnp.broadcast_to(jnp.stack([top, fall])[None], (devices, 2, heads))
+    tops = lax.all_to_all(own_tops, "sp", 0, 0)
+    all_top, all_fall = tops[:, 0], tops[:, 1]
+    index = jnp.arange(devices)
+    between = (index[None, None, :] > jnp.arange(-1, devices)[None, :, None]) & (
+        index[None, None, :] < index[:, None, None]
+    )
+    after = jnp.sum(jnp.where(between[..., None], all_fall[None, None], 0.0), axis=2)
+    reach = jnp.concatenate([jnp.zeros((1, heads), jnp.float32), all_top])[None] + after
+    earlier = jnp.arange(-1, devices)[None, :, None] < index[:, None, None]
+    reach = jnp.where(earlier, reach, -jnp.inf)
+    top_in = jnp.max(reach, axis=1)
+    share = jnp.exp(reach - top_in[:, None])[:, 1:]
+    pieces = lax.all_to_all(
+        jnp.transpose(memory.reshape(heads, devices, rows // devices, columns), (1, 0, 2, 3)),
+        "sp", 0, 0,
+    )
+    sums = jnp.einsum("kjh,jhde->khde", share, pieces, precision=lax.Precision.HIGHEST)
+    back = lax.all_to_all(sums, "sp", 0, 0)
+    memory_in = jnp.transpose(back, (1, 0, 2, 3)).reshape(heads, rows, columns)
+    return (memory_in, lax.dynamic_index_in_dim(top_in, here, 0, False), jnp.zeros_like(fall))
 
 
 def merge_states(earlier, later):
@@ -71,13 +81,7 @@
     device_total, before_block = lax.scan(
         advance, neutral, (block_memory, block_top.T, block_fall.T)
     )
-    incoming = entering_2(device_total, "sp", merge_states, neutral)
-    start_state = (
-        jnp.zeros((local_heads, HEAD_DIM, HEAD_DIM), jnp.float32),
-        jnp.zeros((local_heads,), jnp.float32),
-        jnp.zeros((local_heads,), jnp.float32),
-    )
-    entering = merge_states(start_state, incoming)
+    entering = entering_state(device_total)
     memory_in, top_in, fall_in = merge_states(
         jax.tree.map(lambda member: member[None], entering), before_block
     )
@@ -140,6 +144,34 @@
     factor = lax.rsqrt(squares / D + norm_eps)
     own_norm = lax.dynamic_slice_in_dim(norm_gain, column_index * columns, columns)
     own_normed = (mixed_stream * factor[:, None] * own_norm).astype(jnp.bfloat16)
+    if 2 * own_normed.size * lax.axis_size("tp") < 3 * gate_weight.size:
+        channel = move_tokens(own_normed, gate_weight, up_weight, down_weight)
+    else:
+        channel = move_weights(own_normed, gate_weight, up_weight, down_weight)
+    return mixed_stream + 0.5 * channel
+
+
+def move_tokens(own_normed, gate_weight, up_weight, down_weight):
+    devices = lax.axis_size("sp")
+    rows, units = gate_weight.shape
+    own_units = units // devices
+    weights = jnp.stack([gate_weight.T, up_weight.T, down_weight.T])
+    weights = weights.reshape(3, devices, own_units, rows)
+    weights = lax.all_to_all(weights, "sp", 1, 2)
+    weights = weights.reshape(3, own_units, devices * rows)
+    half = lax.all_gather(own_normed, "sp", axis=0, tiled=True)
+    normed = lax.all_gather(half, "tp", axis=1, tiled=True)
+    gate_acts = jnp.einsum("td,fd->tf", normed, weights[0], preferred_element_type=jnp.float32)
+    up_acts = jnp.einsum("td,fd->tf", normed, weights[1], preferred_element_type=jnp.float32)
+    hidden = (jax.nn.silu(gate_acts) * up_acts).astype(jnp.bfloat16)
+    terms = jnp.einsum("tf,fd->td", hidden, weights[2], preferred_element_type=jnp.float32)
+    terms = lax.psum_scatter(
+        terms.astype(jnp.bfloat16), "tp", scatter_dimension=1, tiled=True
+    )
+    return lax.psum_scatter(terms, "sp", scatter_dimension=0, tiled=True).astype(jnp.float32)
+
+
+def move_weights(own_normed, gate_weight, up_weight, down_weight):
     normed = lax.all_gather(own_normed, "tp", axis=1, tiled=True)
     gate_acts = jnp.dot(
         normed,
@@ -161,7 +193,7 @@
     channel = lax.psum_scatter(
         channel_terms.astype(jnp.bfloat16), "tp", scatter_dimension=0, tiled=True
     ).astype(jnp.float32)
-    return mixed_stream + 0.5 * channel.T
+    return channel.T
 
 
 def solution(mesh):

time: 549 us -> 341 us (0.62)
  waiting for transfers between devices: 396 us -> 199 us
  blocking collectives: 87 us -> 70.7 us
  other arithmetic: 24.1 us -> 10.1 us
  starting transfers between devices: 0.19 us -> 12.1 us
  local copies, waits for them, and re-layouts: 3.43 us -> 12.9 us
    all_gather x4 -> x2, waiting for transfers between devices: 388 us -> 73.6 us  [the longest x1 73.6 us: move_tokens(): half = lax.all_gather(own_normed, 'sp', axis=0, tiled=True)]
    reduce_scatter x1 -> x2, waiting for transfers between devices: 6.26 us -> 112 us  [the longest x1 98.7 us: move_tokens(): lax.psum_scatter(terms, 'sp', scatter_dimension=0, tiled=True)]
    all_to_all x0 -> x2, blocking collectives: none -> 66.3 us  [the longest x1 54.4 us: move_tokens(): weights = lax.all_to_all(weights, 'sp', 1, 2)]
    unnamed x1 -> x0, blocking collectives: 44.2 us -> none
    all_gather x2 -> x0, blocking collectives: 38.3 us -> none  [the longest x1 36.1 us: entering_2(): everything = jax.tree.map(lambda part: lax.all_gather(part, axis), array)]
    select_n x32 -> x0, other arithmetic: 17.5 us -> none  [step(): return jax.tree.map(lambda a, b: jnp.where(reached, a, b), new, before)]
    all_to_all x0 -> x2, waiting for transfers between devices: none -> 12.8 us  [the longest x1 8.61 us: entering_state(): back = lax.all_to_all(sums, 'sp', 0, 0)]
    all_to_all x0 -> x2, starting transfers between devices: none -> 11.9 us  [the longest x1 8.34 us: entering_state(): tops = lax.all_to_all(own_tops, 'sp', 0, 0)]
  transfers between devices with their start and end apart: 5 -> 6, of which waited for: 4 -> 5; matrix products, arithmetic and copies ran while one was open for 5% -> 4% of each run, Pallas kernels for 0% -> 0%
where the time goes in v1:
time: 341 us; the launch traced here: 340 us
  waiting for transfers between devices  199 us (58%)
  blocking collectives  70.7 us (21%)
  matrix products  22 us (6%)
  between operations  13.3 us (4%)
  local copies, waits for them, and re-layouts  12.9 us (4%)
  starting transfers between devices  12.1 us (4%)
  other arithmetic  10.1 us (3%)
    reduce_scatter x1, waiting for transfers between devices, move_tokens(): lax.psum_scatter(terms, 'sp', scatter_dimension=0, tiled=True)  98.7 us
    all_gather x1, waiting for transfers between devices, move_tokens(): half = lax.all_gather(own_normed, 'sp', axis=0, tiled=True)  73.6 us
    all_to_all x1, blocking collectives, move_tokens(): weights = lax.all_to_all(weights, 'sp', 1, 2)  54.4 us
    reduce_scatter x1, waiting for transfers between devices, move_tokens(): lax.psum_scatter(terms.astype(jnp.bfloat16), 'tp', scatter_dimension=1, t...  13.6 us
    dot_general x1, matrix products, move_tokens(): jnp.einsum('tf,fd->td', hidden, weights[2], preferred_element_type=jnp.fl...  12.3 us
    all_to_all x1, blocking collectives, entering_state(): lax.all_to_all(jnp.transpose(memory.reshape(heads, devices, rows // devic...  11.9 us
    all_to_all x1, waiting for transfers between devices, entering_state(): back = lax.all_to_all(sums, 'sp', 0, 0)  8.61 us
    all_to_all x1, starting transfers between devices, entering_state(): tops = lax.all_to_all(own_tops, 'sp', 0, 0)  8.34 us
  transfers between devices with their start and end apart: 6, of which 5 were waited for; matrix products, arithmetic and copies ran while one was open for 4% of the time, Pallas kernels for 0%

profile of v1, /device:TPU:0, one launch (start us, length us, event | category | flops | bytes accessed | tf_op | source)
XLA Modules:
  0.0 339.9 jit_solution(915699007568806377)
XLA Ops:
  6.5 0.9 fusion.53
  7.4 1.2 reduce_window_sum.13
  8.6 0.1 slice.31
  8.7 0.1 copy.154
  8.8 0.1 copy.127
  8.9 0.9 fusion.60
  9.8 0.1 copy.128
  9.9 0.1 pad_maximum_fusion.1
  9.9 0.1 copy.130
  10.0 0.6 broadcast_in_dim.92
  10.7 8.3 %all-to-all-start = ((f32[16,2,4]{2,1,0:T(2,128)}), f32[16,2,4]{2,1,0:T(2,128)S(1)}, u32[]{:S(2)}, u32[]{:S(2)}) async-start(f32[16,2,4]{2,1,0:T(2,128)} %broadcast_in_dim.92), calls=%async_computation | async-start | bytes 32768 | tf_op jit(solution)/shard_map/all_to_all | solution.py:20
  19.1 0.1 broadcast_and_fusion
  19.2 0.9 select_reduce_fusion.1
  20.1 1.0 copy.155
  21.2 1.0 copy.156
  22.2 4.1 %all-to-all-done = f32[16,2,4]{2,1,0:T(2,128)S(1)} async-done(((f32[16,2,4]{2,1,0:T(2,128)}), f32[16,2,4]{2,1,0:T(2,128)S(1)}, u32[]{:S(2)}, u32[]{:S(2)}) %all-to-all-start) | async-done | bytes 544 | tf_op jit(solution)/shard_map/all_to_all | solution.py:20
  26.4 0.1 copy.131
  26.4 0.1 concatenate.4
  26.5 0.1 copy.132
  26.6 0.2 select_reduce_fusion
  26.8 0.1 fusion.61
  26.9 0.2 fusion.48
  27.1 0.8 multiply_bitcast_fusion
  27.9 0.2 convolution_bitcast_fusion.3
  28.1 0.1 fusion.20
  28.2 11.9 %all_to_all.30 = f32[16,4,8,128]{3,2,1,0:T(8,128)S(1)} all-to-all(f32[16,4,8,128]{3,2,1,0:T(8,128)S(1)} %fusion.20), channel_id=1, replica_groups=mesh['sp'=16,'tp'=2] {'sp'}, dimensions={0} | all-to-all | bytes 524288 | tf_op jit(solution)/shard_map/all_to_all | solution.py:32
  40.1 0.5 convolution_bitcast_fusion.2
  40.6 0.8 copy.138
  41.4 3.5 %all-to-all-start.2 = ((f32[16,4,8,128]{3,2,1,0:T(8,128)}), f32[16,4,8,128]{3,2,1,0:T(8,128)S(1)}, u32[]{:S(2)}, u32[]{:S(2)}) async-start(f32[16,4,8,128]{3,2,1,0:T(8,128)} %copy.138), calls=%async_computation.2 | async-start | bytes 524288 | tf_op jit(solution)/shard_map/all_to_all | solution.py:37
  45.0 0.0 all-gather.3.cloned.1.call-start
  45.0 0.1 dynamic-slice_bitcast_fusion
  45.1 0.4 convolution_bitcast_fusion.1
  45.5 0.1 fusion.52
  45.6 8.6 %all-to-all-done.2 = f32[16,4,8,128]{3,2,1,0:T(8,128)S(1)} async-done(((f32[16,4,8,128]{3,2,1,0:T(8,128)}), f32[16,4,8,128]{3,2,1,0:T(8,128)S(1)}, u32[]{:S(2)}, u32[]{:S(2)}) %all-to-all-start.2) | async-done | bytes 262176 | tf_op jit(solution)/shard_map/all_to_all | solution.py:37
  54.2 0.5 multiply_reduce_fusion.1
  54.7 0.0 dynamic-slice-start
  54.7 0.1 multiply_convert_fusion.1
  54.8 2.0 all_gather.9
  56.8 0.5 multiply_reduce_fusion
  57.4 2.5 psum.7
  59.9 0.8 multiply_convert_fusion
  60.7 0.0 all-gather.3.cloned.1.call-update
  60.7 0.0 all-gather.5.cloned.1.call-start
  60.7 73.6 %all-gather.3.cloned.1.call-done = bf16[2048,1024]{1,0:T(8,128)(2,1)} async-done(((bf16[128,1024]{1,0:T(8,128)(2,1)}), bf16[2048,1024]{1,0:T(8,128)(2,1)}) %all-gather.3.cloned.1.call-update) | async-done | bytes 4194320 | tf_op jit(solution)/shard_map/all_gather | solution.py:162
  134.4 0.0 all-gather.5.cloned.1.call-update
  134.4 0.0 reduce-scatter.3.cloned.1.call-start
  134.4 1.5 copy.145
  135.9 2.3 copy.146
  138.2 2.3 copy.147
  140.4 1.8 pad_maximum_fusion
  142.2 0.1 copy.148
  142.4 54.4 %all_to_all.31 = bf16[3,16,176,1,128]{4,2,3,0,1:T(8,128)(2,1)S(1)} all-to-all(bf16[3,16,176,1,128]{4,2,3,0,1:T(8,128)(2,1)S(1)} %copy.148), channel_id=1, replica_groups=mesh['sp'=16,'tp'=2] {'sp'}, dimensions={1} | all-to-all | bytes 4325376 | tf_op jit(solution)/shard_map/all_to_all | solution.py:160
  196.7 0.1 fusion.63
  196.9 0.2 copy.150
  197.1 1.1 copy.151
  198.2 1.1 copy.149
  199.2 7.6 %fusion.11 = f32[2048,176]{0,1:T(8,128)} fusion(bf16[2048,2048]{1,0:T(8,128)(2,1)} %all-gather.5.cloned.1.call-done, bf16[22,8,16,128]{3,2,1,0:T(8,128)(2,1)} %bitcast.129), kind=kOutput, calls=%fused_computation.18 | convolution fusion | flops 1476395008 | bytes 10551296 | tf_op jit(solution)/shard_map/td,fd->tf/dot_general | solution.py:164
  206.8 12.3 %convolution_convert_fusion = bf16[2048,2048]{1,0:T(8,128)(2,1)} fusion(bf16[2048,2048]{1,0:T(8,128)(2,1)} %all-gather.5.cloned.1.call-done, f32[2048,176]{0,1:T(8,128)} %fusion.11, bf16[22,8,16,128]{3,2,1,0:T(8,128)(2,1)} %bitcast.128, bf16[22,8,16,128]{3,2,1,0:T(8,128)(2,1)S(1)} %bitcast.127), kind=kOutput, calls=%fused_computation | convolution fusion | flops 2959147008 | bytes 19660800 | tf_op jit(solution)/shard_map/tf,fd->td/dot_general | solution.py:167
  219.1 0.0 reduce-scatter.3.cloned.1.call-update
  219.1 0.0 reduce-scatter.5.cloned.1.call-start
  219.2 13.6 %reduce-scatter.3.cloned.1.call-done = bf16[2048,1024]{1,0:T(8,128)(2,1)} async-done(((bf16[2048,2048]{1,0:T(8,128)(2,1)}), bf16[2048,1024]{1,0:T(8,128)(2,1)}) %reduce-scatter.3.cloned.1.call-update) | async-done | bytes 4194320 | tf_op jit(solution)/shard_map/reduce_scatter | solution.py:168
  232.8 0.0 reduce-scatter.5.cloned.1.call-update
  232.9 98.7 %reduce-scatter.5.cloned.1.call-done = bf16[128,1024]{1,0:T(8,128)(2,1)} async-done(((bf16[2048,1024]{1,0:T(8,128)(2,1)}), bf16[128,1024]{1,0:T(8,128)(2,1)}) %reduce-scatter.5.cloned.1.call-update) | async-done | bytes 262160 | tf_op jit(solution)/shard_map/reduce_scatter | solution.py:171
  331.6 1.8 multiply_add_fusion
  (22 shorter events, 0.1 us)
Async XLA Ops:
  6.5 50.3 %copy-start = (bf16[1024,1024]{1,0:T(8,128)(2,1)S(1)}, bf16[1024,1024]{1,0:T(8,128)(2,1)}, u32[]{:S(2)}) copy-start(bf16[1024,1024]{1,0:T(8,128)(2,1)} %param.19) | copy-start | bytes 6291460
  6.5 38.6 %copy-start.3 = (f32[4,128]{1,0:T(4,128)S(1)}, f32[4,128]{1,0:T(4,128)}, u32[]{:S(2)}) copy-start(f32[4,128]{1,0:T(4,128)} %param.15) | copy-start | bytes 6148
  6.5 38.5 %copy-start.4 = (f32[1024]{0:T(1024)S(1)}, f32[1024]{0:T(1024)}, u32[]{:S(2)}) copy-start(f32[1024]{0:T(1024)} %param.18) | copy-start | bytes 12292
  6.5 38.6 %copy-start.2 = (bf16[128,512]{1,0:T(8,128)(2,1)S(1)}, bf16[128,512]{1,0:T(8,128)(2,1)}, u32[]{:S(2)}) copy-start(bf16[128,512]{1,0:T(8,128)(2,1)} %param.12) | copy-start | bytes 393220
  10.7 15.7 %all-to-all-start = ((f32[16,2,4]{2,1,0:T(2,128)}), f32[16,2,4]{2,1,0:T(2,128)S(1)}, u32[]{:S(2)}, u32[]{:S(2)}) async-start(f32[16,2,4]{2,1,0:T(2,128)} %broadcast_in_dim.92), calls=%async_computation | async-start | bytes 32768 | tf_op jit(solution)/shard_map/all_to_all | solution.py:20
  40.1 16.7 %copy-start.1 = (bf16[128,1024]{1,0:T(8,128)(2,1)S(1)}, bf16[128,1024]{1,0:T(8,128)(2,1)}, u32[]{:S(2)}) copy-start(bf16[128,1024]{1,0:T(8,128)(2,1)} %param.17) | copy-start | bytes 786436
  41.4 12.8 %all-to-all-start.2 = ((f32[16,4,8,128]{3,2,1,0:T(8,128)}), f32[16,4,8,128]{3,2,1,0:T(8,128)S(1)}, u32[]{:S(2)}, u32[]{:S(2)}) async-start(f32[16,4,8,128]{3,2,1,0:T(8,128)} %copy.138), calls=%async_computation.2 | async-start | bytes 524288 | tf_op jit(solution)/shard_map/all_to_all | solution.py:37
  45.0 89.4 %all-gather.3.cloned.1.call-start = ((), (), s32[]{:S(2)}) async-start(), calls=%async_computation.6 | async-start | bytes 4456448 | tf_op jit(solution)/shard_map/all_gather | solution.py:162
  54.7 5.2 %dynamic-slice-start = ((f32[2048]{0:T(1024)}, s32[]{:T(128)}), f32[1024]{0:T(1024)S(1)}, s32[]{:S(2)}) async-start(f32[2048]{0:T(1024)} %param.20, s32[]{:T(128)} %select_n.44), calls=%async_computation.10 | async-start | bytes 8704 | tf_op jit(solution)/shard_map/dynamic_slice | solution.py:145
  60.7 138.5 %all-gather.5.cloned.1.call-start = ((), (), s32[]{:S(2)}) async-start(), calls=%async_computation.7 | async-start | bytes 12582912 | tf_op jit(solution)/shard_map/all_gather | solution.py:163
  134.4 98.4 %reduce-scatter.3.cloned.1.call-start = ((), (), s32[]{:S(2)}) async-start(), calls=%async_computation.8 | async-start | bytes 12582912 | tf_op jit(solution)/shard_map/reduce_scatter | solution.py:168
  219.1 112.4 %reduce-scatter.5.cloned.1.call-start = ((), (), s32[]{:S(2)}) async-start(), calls=%async_computation.9 | async-start | bytes 4456448 | tf_op jit(solution)/shard_map/reduce_scatter | solution.py:171
Sparse Core Ops, SparseCore 0:
  60.8 73.5 all-gather.2
  135.9 18.4 all-gather.4
  219.3 13.5 reduce-scatter.2
  235.0 96.5 reduce-scatter.4
